TPU v7x, 32 devices: a whole 2x2x4 slice. The times are simulated.
32 devices in a mesh: kv: 8 (over z, y), tp: 4 (over x, core).
Axes of the slice: x: 2, y: 2, z: 4, core: 2. Of those that a mesh axis runs over, the one named last changes fastest.
Arguments:
- hidden_rows: bfloat16 [128, 4096], P('kv', 'tp'), may hold values from -16 to 16
- carried_state: float32 [128, 524288], P('kv', 'tp'), may hold values from -6 to 6
- norm_gain: bfloat16 [4096], replicated, may hold values from 0.099609375 to 1.8984375
- w_query: bfloat16 [4096, 2048], P('kv', 'tp'), may hold values from -0.09375 to 0.09375
- w_key: bfloat16 [4096, 2048], P('kv', 'tp'), may hold values from -0.09375 to 0.09375
- w_decay: bfloat16 [4096, 2048], P('kv', 'tp'), may hold values from -0.375 to 0.375
- w_value: bfloat16 [4096, 4096], P('kv', 'tp'), may hold values from -0.09375 to 0.09375
- w_gate: bfloat16 [4096, 4096], P('kv', 'tp'), may hold values from -0.09375 to 0.09375
- decay_bias: float32 [2048], P('tp'), may hold values from -32 to 8
- head_gain: bfloat16 [256], replicated, may hold values from 0.099609375 to 1.8984375
- w_out: bfloat16 [4096, 4096], P('tp', 'kv'), may hold values from -0.09375 to 0.09375
- mlp_gain: bfloat16 [4096], P('tp'), may hold values from 0.099609375 to 1.8984375
- w_up: bfloat16 [4096, 16384], P('tp', 'kv'), may hold values from -0.09375 to 0.09375
- w_down: bfloat16 [16384, 4096], P('kv', 'tp'), may hold values from -0.046875 to 0.046875
Outputs:
- updated_rows: bfloat16 [128, 4096], P('kv', 'tp')
- new_state: float32 [128, 524288], P('kv', 'tp')
All inputs are finite; a program needn't handle non-finite values.
Results may differ from a plain program's by a relative error of at most 0.025.
Values may be sent and summed in bfloat16 or wider, within the bound.
A program may use at most 128 MiB of HBM per device.

v0:
```python
import jax
import jax.numpy as jnp
from jax import lax
from jax.sharding import PartitionSpec as P

D = 4096
DK = 128
DV = 256


epsilon = 1e-06
decay_normalizer = 16.0


def body(
    hidden_rows,
    carried_state,
    norm_gain,
    w_query,
    w_key,
    w_decay,
    w_value,
    w_gate,
    decay_bias,
    head_gain,
    w_out,
    mlp_gain,
    w_up,
    w_down,
):
    seq_rows = hidden_rows.shape[0]
    heads_here = decay_bias.shape[0] // DK
    gathered = lax.all_gather(hidden_rows, "tp", axis=1, tiled=True)
    whole_inputs = gathered.astype(jnp.float32)
    normed = (
        whole_inputs
        * lax.rsqrt(jnp.mean(whole_inputs * whole_inputs, axis=-1, keepdims=True) + epsilon)
        * norm_gain.astype(jnp.float32)
    ).astype(jnp.bfloat16)
    weights = (w_query, w_key, w_decay, w_value, w_gate)
    feature_blocks = lax.all_to_all(normed, "kv", split_axis=1, concat_axis=0, tiled=True)
    joined = jnp.concatenate(weights, axis=1)
    block_rows = feature_blocks
    summed = lax.psum_scatter(
        jnp.dot(block_rows, joined, preferred_element_type=jnp.float32).astype(jnp.bfloat16),
        "kv",
        scatter_dimension=0,
        tiled=True,
    ).astype(jnp.float32)
    projected = []
    offset = 0
    for weight in weights:
        projected.append(summed[:, offset : offset + weight.shape[1]])
        offset = offset + weight.shape[1]
    queries, keys_new, decay_pre, values, out_gate = [
        item.astype(jnp.bfloat16) for item in projected
    ]
    log_decay = jax.nn.log_sigmoid(decay_pre.astype(jnp.float32) + decay_bias) / decay_normalizer
    log_decay = log_decay.reshape(seq_rows, heads_here, DK)
    carried = carried_state.reshape(seq_rows, heads_here, DK, DV)
    key_heads = keys_new.astype(jnp.float32).reshape(seq_rows, heads_here, DK)
    value_heads = values.astype(jnp.float32).reshape(seq_rows, heads_here, DV)
    new_state = (
        jnp.exp(log_decay)[..., None] * carried + key_heads[..., None] * value_heads[..., None, :]
    )
    query_heads = queries.astype(jnp.float32).reshape(seq_rows, heads_here, DK) * DK ** (-0.5)
    head_out = jnp.einsum("bhk,bhkv->bhv", query_heads, new_state, precision=lax.Precision.HIGHEST)
    gate_heads = out_gate.astype(jnp.float32).reshape(seq_rows, heads_here, DV)
    mixed = head_out * lax.rsqrt(jnp.mean(head_out * head_out, axis=-1, keepdims=True) + epsilon)
    mixed = (mixed * head_gain.astype(jnp.float32) * jax.nn.silu(gate_heads)).astype(jnp.bfloat16)
    mixed = mixed.reshape(seq_rows, heads_here * DV)
    partial_out = jnp.dot(
        mixed, lax.all_gather(w_out, "kv", axis=1, tiled=True), preferred_element_type=jnp.float32
    ).astype(jnp.bfloat16)
    attn_out = lax.psum_scatter(
        partial_out.astype(jnp.float32).astype(jnp.bfloat16), "tp", scatter_dimension=1, tiled=True
    )
    residual = (hidden_rows.astype(jnp.float32) + attn_out.astype(jnp.float32)).astype(jnp.bfloat16)
    resid_float = residual.astype(jnp.float32)
    total_squares = lax.psum(jnp.sum(resid_float * resid_float, axis=-1), "tp")
    row_scale = lax.rsqrt(total_squares / D + epsilon)
    mlp_input = (resid_float * row_scale[:, None] * mlp_gain.astype(jnp.float32)).astype(
        jnp.bfloat16
    )
    up_partial = jnp.dot(
        lax.all_gather(mlp_input, "kv", axis=0, tiled=True),
        w_up,
        preferred_element_type=jnp.float32,
    ).astype(jnp.bfloat16)
    up_sum = lax.psum(up_partial.astype(jnp.float32).astype(jnp.bfloat16), "tp").astype(jnp.float32)
    activation = jnp.square(jax.nn.relu(up_sum)).astype(jnp.bfloat16)
    block_rows = activation
    mlp_total = lax.psum_scatter(
        jnp.dot(block_rows, w_down, preferred_element_type=jnp.float32).astype(jnp.bfloat16),
        "kv",
        scatter_dimension=0,
        tiled=True,
    )
    updated_rows = (resid_float + mlp_total.astype(jnp.float32)).astype(jnp.bfloat16)
    return (updated_rows, new_state.reshape(seq_rows, heads_here * DK * DV))


def solution(mesh):
    return jax.shard_map(
        body,
        mesh=mesh,
        in_specs=(
            P("kv", "tp"),
            P("kv", "tp"),
            P(),
            P("kv", "tp"),
            P("kv", "tp"),
            P("kv", "tp"),
            P("kv", "tp"),
            P("kv", "tp"),
            P("tp"),
            P(),
            P("tp", "kv"),
            P("tp"),
            P("tp", "kv"),
            P("kv", "tp"),
        ),
        out_specs=(P("kv", "tp"), P("kv", "tp")),
        check_vma=False,
    )
```

profile of v0, /device:TPU:0, one launch (start us, length us, event | category | flops | bytes accessed | tf_op | source)
XLA Modules:
  0.0 400.0 jit_solution(15394609910348088016)
XLA Ops:
  7.2 6.7 %all_gather.9 = bf16[16,4096]{1,0:T(8,128)(2,1)S(1)} all-gather(bf16[16,1024]{1,0:T(8,128)(2,1)} %param.14), channel_id=1, replica_groups=mesh['kv'=8,'tp'=4] {'tp'}, dimensions={1}, use_global_device_ids=true | all-gather | bytes 163840 | tf_op jit(solution)/shard_map/all_gather | solution.py:33
  15.5 6.2 %all-to-all-start = ((bf16[16,8,512]{2,0,1:T(8,128)(2,1)}), bf16[16,8,512]{2,0,1:T(8,128)(2,1)S(1)}, u32[]{:S(2)}, u32[]{:S(2)}) async-start(bf16[16,8,512]{2,0,1:T(8,128)(2,1)} %bitcast.37), calls=%async_computation | async-start | bytes 262144 | tf_op jit(solution)/shard_map/all_to_all | solution.py:41
  21.8 1.9 constant_dynamic-update-slice_fusion.4
  23.6 1.9 constant_dynamic-update-slice_fusion.3
  25.5 1.9 constant_dynamic-update-slice_fusion.2
  27.4 2.3 constant_dynamic-update-slice_fusion.1
  29.6 2.3 constant_dynamic-update-slice_fusion
  31.9 3.7 convolution_convert_fusion
  36.5 9.3 %copy.21 = f32[2,8,512,256]{3,2,1,0:T(8,128)} copy(f32[2,8,512,256]{3,1,2,0:T(8,128)} %bitcast.41) | data formatting | bytes 16777216
  45.7 55.1 %reduce-scatter.4.cloned.1.call-done = bf16[16,3584]{1,0:T(8,128)(2,1)} async-done(((bf16[128,3584]{1,0:T(8,128)(2,1)}), bf16[16,3584]{1,0:T(8,128)(2,1)}) %reduce-scatter.4.cloned.1.call-update) | async-done | bytes 114704 | tf_op jit(solution)/shard_map/reduce_scatter | solution.py:44
  103.2 7.5 %fusion = f32[16,4,1,256]{3,2,1,0:T(1,128)S(1)} fusion(f32[16,4,128,1]{2,3,1,0:T(1,128)S(1)} %bitcast.47, f32[16,4,128,256]{3,2,1,0:T(8,128)} %bitcast.38, f32[16,4,128]{2,1,0:T(4,128)S(1)} %exp.21, f32[16,4,256]{2,1,0:T(4,128)S(1)} %reshape.62, f32[16,4,128]{2,1,0:T(4,128)S(1)} %reshape.61), kind=kOutput, calls=%fused_computation.1 | convolution fusion | flops 31457280 | bytes 8617984 | tf_op jit(solution)/shard_map/bhk,bhkv->bhv/dot_general | solution.py:67
  111.0 115.8 %all-gather.2.cloned.1.call-done = bf16[1024,4096]{1,0:T(8,128)(2,1)} async-done(((bf16[1024,512]{1,0:T(8,128)(2,1)}), bf16[1024,4096]{1,0:T(8,128)(2,1)}) %all-gather.2.cloned.1.call-update) | async-done | bytes 8388624 | tf_op jit(solution)/shard_map/all_gather | solution.py:73
  226.8 5.2 %convolution_convert_fusion.1 = bf16[16,4096]{1,0:T(8,128)(2,1)} fusion(bf16[16,1024]{1,0:T(8,128)(2,1)S(1)} %bitcast.46, bf16[1024,4096]{1,0:T(8,128)(2,1)} %all-gather.2.cloned.1.call-done), kind=kOutput, calls=%fused_computation.5 | convolution fusion | flops 134283264 | bytes 8552448 | tf_op jit(solution)/shard_map/dot_general | solution.py:72
  232.2 17.9 %reduce-scatter.6.cloned.1.call-done = bf16[16,1024]{1,0:T(8,128)(2,1)} async-done(((bf16[16,4096]{1,0:T(8,128)(2,1)}), bf16[16,1024]{1,0:T(8,128)(2,1)}) %reduce-scatter.6.cloned.1.call-update) | async-done | bytes 32784 | tf_op jit(solution)/shard_map/reduce_scatter | solution.py:75
  250.9 5.8 %psum.14 = f32[16]{0:T(128)S(1)} all-reduce(f32[16]{0:T(128)S(1)} %fusion.9), channel_id=1, replica_groups=mesh['kv'=8,'tp'=4] {'tp'}, use_global_device_ids=true, to_apply=%region_5.6 | all-reduce | flops 16 | bytes 128 | tf_op jit(solution)/shard_map/psum | solution.py:80
  257.5 31.1 %all_gather.11 = bf16[128,1024]{1,0:T(8,128)(2,1)S(1)} all-gather(bf16[16,1024]{1,0:T(8,128)(2,1)S(1)} %fusion.11), channel_id=1, replica_groups=mesh['kv'=8,'tp'=4] {'kv'}, dimensions={0}, use_global_device_ids=true | all-gather | bytes 294912 | tf_op jit(solution)/shard_map/all_gather | solution.py:86
  288.6 3.8 convolution_convert_fusion.2
  294.0 8.3 %copy.24 = f32[2,8,512,256]{3,1,2,0:T(8,128)} copy(f32[2,8,512,256]{3,2,1,0:T(8,128)S(1)} %bitcast.39) | data formatting | bytes 16777216
  303.5 8.1 %copy.23 = f32[2,8,512,256]{3,1,2,0:T(8,128)} copy(f32[2,8,512,256]{3,2,1,0:T(8,128)S(1)} %bitcast.40) | data formatting | bytes 16777216
  311.5 14.4 %all-reduce.2.cloned.1.call-done = bf16[128,2048]{1,0:T(8,128)(2,1)} async-done(((bf16[128,2048]{1,0:T(8,128)(2,1)}), bf16[128,2048]{1,0:T(8,128)(2,1)}) %all-reduce.2.cloned.1.call-update) | async-done | bytes 524304 | tf_op jit(solution)/shard_map/psum | solution.py:90
  325.9 3.8 convolution_convert_fusion.3
  329.7 12.4 %multiply_add_fusion = f32[16,131072]{1,0:T(8,128)} fusion(f32[16,131072]{1,0:T(8,128)} %bitcast.42, f32[16,131072]{1,0:T(8,128)} %bitcast.43, f32[16,131072]{1,0:T(8,128)} %param.15), kind=kLoop, calls=%fused_computation | loop fusion | flops 4194304 | bytes 33554432 | tf_op jit(solution)/shard_map/add | solution.py:64
  342.1 50.0 %reduce-scatter.8.cloned.1.call-done = bf16[16,1024]{1,0:T(8,128)(2,1)} async-done(((bf16[128,1024]{1,0:T(8,128)(2,1)}), bf16[16,1024]{1,0:T(8,128)(2,1)}) %reduce-scatter.8.cloned.1.call-update) | async-done | bytes 32784 | tf_op jit(solution)/shard_map/reduce_scatter | solution.py:93
  392.1 1.4 fusion.12
  (45 shorter events, 9.6 us)
Async XLA Ops:
  15.5 16.4 %all-to-all-start = ((bf16[16,8,512]{2,0,1:T(8,128)(2,1)}), bf16[16,8,512]{2,0,1:T(8,128)(2,1)S(1)}, u32[]{:S(2)}, u32[]{:S(2)}) async-start(bf16[16,8,512]{2,0,1:T(8,128)(2,1)} %bitcast.37), calls=%async_computation | async-start | bytes 262144 | tf_op jit(solution)/shard_map/all_to_all | solution.py:41
  21.7 79.1 %reduce-scatter.4.cloned.1.call-start = ((), (), s32[]{:S(2)}) async-start(), calls=%async_computation.4 | async-start | bytes 1032192 | tf_op jit(solution)/shard_map/reduce_scatter | solution.py:44
  35.6 191.2 %all-gather.2.cloned.1.call-start = ((), (), s32[]{:S(2)}) async-start(), calls=%async_computation.5 | async-start | bytes 9437184 | tf_op jit(solution)/shard_map/all_gather | solution.py:73
  36.4 213.7 %reduce-scatter.6.cloned.1.call-start = ((), (), s32[]{:S(2)}) async-start(), calls=%async_computation.6 | async-start | bytes 163840 | tf_op jit(solution)/shard_map/reduce_scatter | solution.py:75
  36.4 9.3 %copy-start.4 = (bf16[256]{0:T(256)(128)(2,1)S(1)}, bf16[256]{0:T(256)(128)(2,1)}, u32[]{:S(2)}) copy-start(bf16[256]{0:T(256)(128)(2,1)} %param.23) | copy-start | bytes 1540
  36.4 65.2 %copy-start.2 = (f32[512]{0:T(512)S(1)}, f32[512]{0:T(512)}, u32[]{:S(2)}) copy-start(f32[512]{0:T(512)} %param.22) | copy-start | bytes 6148
  110.8 121.4 %copy-start.3 = (bf16[1024]{0:T(1024)(128)(2,1)S(1)}, bf16[1024]{0:T(1024)(128)(2,1)}, u32[]{:S(2)}) copy-start(bf16[1024]{0:T(1024)(128)(2,1)} %param.25) | copy-start | bytes 6148
  110.8 139.3 %copy-start = (bf16[16,1024]{1,0:T(8,128)(2,1)S(1)}, bf16[16,1024]{1,0:T(8,128)(2,1)}, u32[]{:S(2)}) copy-start(bf16[16,1024]{1,0:T(8,128)(2,1)} %param.14) | copy-start | bytes 98308
  232.1 93.8 %all-reduce.2.cloned.1.call-start = ((), (), s32[]{:S(2)}) async-start(), calls=%async_computation.7 | async-start | bytes 1048576 | tf_op jit(solution)/shard_map/psum | solution.py:90
  292.5 99.6 %reduce-scatter.8.cloned.1.call-start = ((), (), s32[]{:S(2)}) async-start(), calls=%async_computation.8 | async-start | bytes 294912 | tf_op jit(solution)/shard_map/reduce_scatter | solution.py:93
  329.7 62.4 %copy-start.1 = (bf16[16,1024]{1,0:T(8,128)(2,1)S(1)}, bf16[16,1024]{1,0:T(8,128)(2,1)}, u32[]{:S(2)}) copy-start(bf16[16,1024]{1,0:T(8,128)(2,1)} %reduce-scatter.6.cloned.1.call-done) | copy-start | bytes 98308
Sparse Core Ops, SparseCore 0:
  35.8 65.0 reduce-scatter.3
  102.8 123.9 all-gather.1
  232.2 17.7 reduce-scatter.5
  292.6 33.2 all-reduce.1
  329.8 62.2 reduce-scatter.7
where the time goes:
time: 401 us; the launch traced here: 400 us
  waiting for transfers between devices  254 us (63%)
  blocking collectives  43.6 us (11%)
  local copies, waits for them, and re-layouts  37.8 us (9%)
  matrix products  24.1 us (6%)
  other arithmetic  20.2 us (5%)
  between operations  13.9 us (3%)
  starting transfers between devices  6.6 us (2%)
    all_gather x1, waiting for transfers between devices, body(): lax.all_gather(w_out, 'kv', axis=1, tiled=True)  116 us
    reduce_scatter x1, waiting for transfers between devices, body(): lax.psum_scatter(jnp.dot(block_rows, joined, preferred_element_type=jnp.f...  55.1 us
    reduce_scatter x1, waiting for transfers between devices, body(): lax.psum_scatter(jnp.dot(block_rows, w_down, preferred_element_type=jnp.f...  50 us
    unnamed x18, local copies, waits for them, and re-layouts  33.5 us
    all_gather x1, blocking collectives, body(): lax.all_gather(mlp_input, 'kv', axis=0, tiled=True)  31.1 us
    reduce_scatter x1, waiting for transfers between devices, body(): lax.psum_scatter(partial_out.astype(jnp.float32).astype(jnp.bfloat16), 't...  17.9 us
    psum x1, waiting for transfers between devices, body(): lax.psum(up_partial.astype(jnp.float32).astype(jnp.bfloat16), 'tp')  14.4 us
    add x1, other arithmetic, body(): jnp.exp(log_decay)[..., None] * carried  12.4 us
  transfers between devices with their start and end apart: 6, of which 5 were waited for; matrix products, arithmetic and copies ran while one was open for 15% of the time, Pallas kernels for 0%

commit v1 on v0

v1 whole, which is shorter than its diff:
```python
import functools

import jax
import jax.numpy as jnp
from jax import lax
from jax.experimental import pallas as pl
from jax.experimental.pallas import tpu as pltpu
from jax.sharding import PartitionSpec as P

DK = 128
DV = 256

epsilon = 1e-06
decay_normalizer = 16.0

F32 = jnp.float32
BF16 = jnp.bfloat16
MESH = pl.DeviceIdType.MESH


def remote(src, dst, send_sem, recv_sem, i, j):
    return pltpu.make_async_remote_copy(
        src_ref=src,
        dst_ref=dst,
        send_sem=send_sem,
        recv_sem=recv_sem,
        device_id={"kv": i, "tp": j},
        device_id_type=MESH,
    )


def dot(a, b):
    return jnp.dot(a, b, preferred_element_type=F32)


def project_kernel(
    kv, tp, h_ref, g_ref, w0, w1, w2, w3, w4, o0, o1, o2, o3, o4,
    xbuf, v0, v1, v2, v3, v4, s0, s1, s2, s3, s4, r0, r1, r2, r3, r4,
    ssq, wsem, xs_sem, xr_sem, ss_sem, sr_sem, ps_sem, pr_sem,
):
    i, j = lax.axis_index("kv"), lax.axis_index("tp")
    ratio = kv // tp
    rows = h_ref.shape[0]
    width = xbuf.shape[2]
    owner = i // ratio
    ws, vs, outs = (w0, w1, w2, w3, w4), (v0, v1, v2, v3, v4), (o0, o1, o2, o3, o4)
    sends, recvs = (s0, s1, s2, s3, s4), (r0, r1, r2, r3, r4)
    loads = [pltpu.make_async_copy(w, v, wsem.at[n]) for n, (w, v) in enumerate(zip(ws, vs))]

    hidden_sends = []
    for a in range(ratio):
        for s in range(tp):
            dst_i, dst_j = j * ratio + a, lax.rem(j + s, tp)
            src = h_ref.at[:, pl.ds(a * width, width)]
            copy = remote(
                src, xbuf.at[i], xs_sem.at[a * tp + s], xr_sem.at[i], dst_i, dst_j
            )
            hidden_sends.append((a, s, dst_i, copy))
    for a, s, dst_i, copy in hidden_sends:
        if s:
            copy.start()
        else:
            pl.when(dst_i != i)(copy.start)
    for load in loads:
        load.start()

    hidden = h_ref[...].astype(F32)
    ssq[j] = jnp.broadcast_to(jnp.sum(hidden * hidden, axis=1, keepdims=True), (rows, 128))
    for a, s, dst_i, copy in hidden_sends:
        if not s:

            @pl.when(dst_i == i)
            def _():
                xbuf[i] = h_ref[:, a * width : (a + 1) * width]

    for s in range(kv):
        k = lax.rem(i + s, kv)
        arrive = remote(xbuf.at[k], xbuf.at[k], xs_sem.at[0], xr_sem.at[k], k, owner)
        if s:
            arrive.wait_recv()
        else:
            pl.when(owner != j)(arrive.wait_recv)

    square_sends = [
        remote(ssq.at[j], ssq.at[j], ss_sem.at[s], sr_sem.at[j], i, lax.rem(j + s, tp))
        for s in range(1, tp)
    ]
    gain = g_ref[:, pl.ds(pl.multiple_of(i * width, 128), width)].astype(F32)
    x = (xbuf[...].reshape(kv * rows, width).astype(F32) * gain).astype(BF16)
    part_sends = []
    for n in range(5):
        loads[n].wait()
        part = dot(x, vs[n][...]).astype(BF16)
        sends[n][...] = part.reshape(sends[n].shape)
        for s in range(1, kv):
            k = lax.rem(i + s, kv)
            copy = remote(
                sends[n].at[k], recvs[n].at[i], ps_sem.at[n, s], pr_sem.at[n, i], k, j
            )
            copy.start()
            part_sends.append(copy)
        if n == 0:
            for copy in square_sends:
                copy.start()
    for s in range(1, tp):
        k = lax.rem(j + s, tp)
        remote(ssq.at[k], ssq.at[k], ss_sem.at[0], sr_sem.at[k], i, k).wait_recv()
    total = ssq[0]
    for s in range(1, tp):
        total = total + ssq[s]
    scale = lax.rsqrt(total[:, :1] / (kv * width) + epsilon)
    for n in range(5):
        acc = sends[n][i].astype(F32)
        for s in range(1, kv):
            k = lax.rem(i + s, kv)
            remote(
                recvs[n].at[k], recvs[n].at[k], ps_sem.at[n, 0], pr_sem.at[n, k], k, j
            ).wait_recv()
            acc = acc + recvs[n][k].astype(F32)
        outs[n][...] = (acc * scale).astype(BF16)
    for a, s, dst_i, copy in hidden_sends:
        if s:
            copy.wait_send()
        else:
            pl.when(dst_i != i)(copy.wait_send)
    for copy in square_sends + part_sends:
        copy.wait_send()


def project(kv, tp, hidden_rows, norm_gain, weights):
    rows = hidden_rows.shape[0]
    width = weights[0].shape[0]
    vmem = pl.BlockSpec(memory_space=pltpu.VMEM)
    anywhere = pl.BlockSpec(memory_space=pl.ANY)
    slots = [pltpu.VMEM((kv, rows, w.shape[1]), BF16) for w in weights]
    dma = pltpu.SemaphoreType.DMA
    return pl.pallas_call(
        functools.partial(project_kernel, kv, tp),
        out_shape=[jax.ShapeDtypeStruct((rows, w.shape[1]), BF16) for w in weights],
        in_specs=[vmem] * 2 + [anywhere] * 5,
        out_specs=[vmem] * 5,
        scratch_shapes=[pltpu.VMEM((kv, rows, width), BF16)]
        + [pltpu.VMEM(w.shape, BF16) for w in weights]
        + slots
        + slots
        + [
            pltpu.VMEM((tp, rows, 128), F32),
            dma((5,)),
            dma((kv,)),
            dma((kv,)),
            dma((tp,)),
            dma((tp,)),
            dma((5, kv)),
            dma((5, kv)),
        ],
        compiler_params=pltpu.CompilerParams(
            has_side_effects=True, vmem_limit_bytes=32 * 1024 * 1024
        ),
        name="project",
    )(hidden_rows, norm_gain.reshape(1, -1), *weights)


def tail_kernel(
    kv, tp, mixed_ref, h_ref, g_ref, wo, wu, wd, out_ref,
    vo, vu, vd, mall, psend, precv, resid, rall, ssq, usend, urecv, xsend, xrecv, act, dsend, drecv,
    wsem, ms_sem, mr_sem, ps_sem, pr_sem, rs_sem, rr_sem, ss_sem, sr_sem,
    us_sem, ur_sem, xs_sem, xr_sem, as_sem, ar_sem, ds_sem, dr_sem,
):
    i, j = lax.axis_index("kv"), lax.axis_index("tp")
    ratio = kv // tp
    rows, columns = h_ref.shape
    width = columns // ratio
    owner = i // ratio
    loads = [
        pltpu.make_async_copy(w, v, wsem.at[n])
        for n, (w, v) in enumerate(((wo, vo), (wu, vu), (wd, vd)))
    ]
    sent = []

    def everyone(src_of, dst, send_sem, recv_sem):
        for s in range(1, kv):
            k = lax.rem(i + s, kv)
            copy = remote(src_of(k), dst.at[i], send_sem.at[s], recv_sem.at[i], k, j)
            copy.start()
            sent.append(copy)

    def arrived(dst, send_sem, recv_sem, s):
        k = lax.rem(i + s, kv)
        remote(dst.at[k], dst.at[k], send_sem.at[0], recv_sem.at[k], k, j).wait_recv()
        return k

    everyone(lambda k: mixed_ref, mall, ms_sem, mr_sem)
    for load in loads:
        load.start()
    mall[i] = mixed_ref[...]
    for s in range(1, kv):
        arrived(mall, ms_sem, mr_sem, s)
    loads[0].wait()
    part = dot(mall[...].reshape(kv * rows, mall.shape[2]), vo[...]).astype(BF16)
    psend[...] = part.reshape(psend.shape)

    slot = j * ratio + lax.rem(i, ratio)
    own_send = remote(psend.at[i], precv.at[slot], ps_sem.at[0], pr_sem.at[slot], i, owner)
    for s in range(1, kv):
        k = lax.rem(i + s, kv)
        copy = remote(psend.at[k], precv.at[slot], ps_sem.at[s], pr_sem.at[slot], k, owner)
        copy.start()
        sent.append(copy)
    pl.when(owner != j)(own_send.start)

    @pl.when(owner == j)
    def _():
        precv[slot] = psend[i]

    pieces = []
    for a in range(ratio):
        src_i = j * ratio + a
        attn = None
        for s in range(tp):
            src_j = lax.rem(j + s, tp)
            at = src_j * ratio + a
            arrive = remote(precv.at[at], precv.at[at], ps_sem.at[0], pr_sem.at[at], src_i, src_j)
            if s:
                arrive.wait_recv()
            else:
                pl.when(src_i != i)(arrive.wait_recv)
            term = precv[at].astype(F32)
            attn = term if attn is None else attn + term
        hidden = h_ref[:, a * width : (a + 1) * width].astype(F32)
        piece = (hidden + attn.astype(BF16).astype(F32)).astype(BF16)
        resid[:, a * width : (a + 1) * width] = piece
        piece = piece.astype(F32)
        pieces.append(jnp.sum(piece * piece, axis=1, keepdims=True))

    everyone(lambda k: resid, rall, rs_sem, rr_sem)
    ssq[j] = jnp.broadcast_to(sum(pieces), (rows, 128))
    rall[i] = resid[...]
    loads[1].wait()
    for s in range(1, kv):
        arrived(rall, rs_sem, rr_sem, s)
    for s in range(1, tp):
        copy = remote(ssq.at[j], ssq.at[j], ss_sem.at[s], sr_sem.at[j], i, lax.rem(j + s, tp))
        copy.start()
        sent.append(copy)
    x = (rall[...].reshape(kv * rows, columns).astype(F32) * g_ref[...].astype(F32)).astype(BF16)

    half = vu.shape[1] // 2
    core, across = lax.rem(j, 2), j // 2
    other = 1 - core
    partner = across * 2 + other
    usend[...] = dot(x, vu[:, pl.ds(pl.multiple_of(other * half, 128), half)]).astype(BF16)
    give = remote(usend, urecv, us_sem, ur_sem, i, partner)
    give.start()
    mine = dot(x, vu[:, pl.ds(pl.multiple_of(core * half, 128), half)])
    give.wait_recv()
    mine = (mine + urecv[...].astype(F32)).astype(BF16)
    xsend[...] = mine
    for s in range(1, tp // 2):
        to = lax.rem(across + s, tp // 2)
        copy = remote(
            xsend, xrecv.at[across], xs_sem.at[s], xr_sem.at[across], i, to * 2 + core
        )
        copy.start()
        sent.append(copy)
    loads[2].wait()
    total = xsend[...].astype(F32)
    for s in range(1, tp // 2):
        at = lax.rem(across + s, tp // 2)
        remote(
            xrecv.at[at], xrecv.at[at], xs_sem.at[0], xr_sem.at[at], i, at * 2 + core
        ).wait_recv()
        total = total + xrecv[at].astype(F32)
    act[core] = jnp.square(jnp.maximum(total, 0.0)).astype(BF16)
    share = remote(act.at[core], act.at[core], as_sem, ar_sem.at[core], i, partner)
    share.start()
    down = dot(act[core], vd[pl.ds(pl.multiple_of(core * half, 128), half), :])
    remote(act.at[other], act.at[other], as_sem, ar_sem.at[other], i, partner).wait_recv()
    down = down + dot(act[other], vd[pl.ds(pl.multiple_of(other * half, 128), half), :])
    dsend[...] = down.astype(BF16).reshape(dsend.shape)
    everyone(lambda k: dsend.at[k], drecv, ds_sem, dr_sem)

    for s in range(1, tp):
        k = lax.rem(j + s, tp)
        remote(ssq.at[k], ssq.at[k], ss_sem.at[0], sr_sem.at[k], i, k).wait_recv()
    squares = ssq[0]
    for s in range(1, tp):
        squares = squares + ssq[s]
    scale = lax.rsqrt(squares[:, :1] / (columns * tp) + epsilon)
    acc = dsend[i].astype(F32)
    for s in range(1, kv):
        k = arrived(drecv, ds_sem, dr_sem, s)
        acc = acc + drecv[k].astype(F32)
    acc = (acc * (scale * scale)).astype(BF16)
    out_ref[...] = (resid[...].astype(F32) + acc.astype(F32)).astype(BF16)
    give.wait_send()
    share.wait_send()
    pl.when(owner != j)(own_send.wait_send)
    for copy in sent:
        copy.wait_send()


def tail(kv, tp, mixed, hidden_rows, mlp_gain, w_out, w_up, w_down):
    rows, columns = hidden_rows.shape
    width = w_out.shape[1]
    ratio = kv // tp
    half = w_up.shape[1] // 2
    everything = kv * rows
    vmem = pl.BlockSpec(memory_space=pltpu.VMEM)
    anywhere = pl.BlockSpec(memory_space=pl.ANY)
    dma = pltpu.SemaphoreType.DMA
    return pl.pallas_call(
        functools.partial(tail_kernel, kv, tp),
        out_shape=jax.ShapeDtypeStruct((rows, columns), BF16),
        in_specs=[vmem] * 3 + [anywhere] * 3,
        out_specs=vmem,
        scratch_shapes=[
            pltpu.VMEM(w_out.shape, BF16),
            pltpu.VMEM(w_up.shape, BF16),
            pltpu.VMEM(w_down.shape, BF16),
            pltpu.VMEM((kv, rows, mixed.shape[1]), BF16),
            pltpu.VMEM((kv, rows, width), BF16),
            pltpu.VMEM((tp * ratio, rows, width), BF16),
            pltpu.VMEM((rows, columns), BF16),
            pltpu.VMEM((kv, rows, columns), BF16),
            pltpu.VMEM((tp, rows, 128), F32),
            pltpu.VMEM((everything, half), BF16),
            pltpu.VMEM((everything, half), BF16),
            pltpu.VMEM((everything, half), BF16),
            pltpu.VMEM((tp // 2, everything, half), BF16),
            pltpu.VMEM((2, everything, half), BF16),
            pltpu.VMEM((kv, rows, columns), BF16),
            pltpu.VMEM((kv, rows, columns), BF16),
            dma((3,)),
            dma((kv,)),
            dma((kv,)),
            dma((kv,)),
            dma((tp * ratio,)),
            dma((kv,)),
            dma((kv,)),
            dma((tp,)),
            dma((tp,)),
            dma(()),
            dma(()),
            dma((tp // 2,)),
            dma((tp // 2,)),
            dma(()),
            dma((2,)),
            dma((kv,)),
            dma((kv,)),
        ],
        compiler_params=pltpu.CompilerParams(
            has_side_effects=True, vmem_limit_bytes=32 * 1024 * 1024
        ),
        name="tail",
    )(mixed, hidden_rows, mlp_gain.reshape(1, -1), w_out, w_up, w_down)


def body(
    kv,
    tp,
    hidden_rows,
    carried_state,
    norm_gain,
    w_query,
    w_key,
    w_decay,
    w_value,
    w_gate,
    decay_bias,
    head_gain,
    w_out,
    mlp_gain,
    w_up,
    w_down,
):
    seq_rows = hidden_rows.shape[0]
    heads_here = decay_bias.shape[0] // DK
    queries, keys_new, decay_pre, values, out_gate = project(
        kv, tp, hidden_rows, norm_gain, (w_query, w_key, w_decay, w_value, w_gate)
    )
    log_decay = jax.nn.log_sigmoid(decay_pre.astype(F32) + decay_bias) / decay_normalizer
    log_decay = log_decay.reshape(seq_rows, heads_here, DK)
    carried = carried_state.reshape(seq_rows, heads_here, DK, DV)
    key_heads = keys_new.astype(F32).reshape(seq_rows, heads_here, DK)
    value_heads = values.astype(F32).reshape(seq_rows, heads_here, DV)
    new_state = (
        jnp.exp(log_decay)[..., None] * carried + key_heads[..., None] * value_heads[..., None, :]
    )
    query_heads = queries.astype(F32).reshape(seq_rows, heads_here, DK) * DK ** (-0.5)
    head_out = jnp.einsum("bhk,bhkv->bhv", query_heads, new_state, precision=lax.Precision.HIGHEST)
    gate_heads = out_gate.astype(F32).reshape(seq_rows, heads_here, DV)
    mixed = head_out * lax.rsqrt(jnp.mean(head_out * head_out, axis=-1, keepdims=True) + epsilon)
    mixed = (mixed * head_gain.astype(F32) * jax.nn.silu(gate_heads)).astype(BF16)
    mixed = mixed.reshape(seq_rows, heads_here * DV)
    updated_rows = tail(kv, tp, mixed, hidden_rows, mlp_gain, w_out, w_up, w_down)
    return (updated_rows, new_state.reshape(seq_rows, heads_here * DK * DV))


def solution(mesh):
    return jax.shard_map(
        functools.partial(body, mesh.shape["kv"], mesh.shape["tp"]),
        mesh=mesh,
        in_specs=(
            P("kv", "tp"),
            P("kv", "tp"),
            P(),
            P("kv", "tp"),
            P("kv", "tp"),
            P("kv", "tp"),
            P("kv", "tp"),
            P("kv", "tp"),
            P("tp"),
            P(),
            P("tp", "kv"),
            P("tp"),
            P("tp", "kv"),
            P("kv", "tp"),
        ),
        out_specs=(P("kv", "tp"), P("kv", "tp")),
        check_vma=False,
    )
```

time: 401 us -> 137 us (0.34)
  waiting for transfers between devices: 254 us -> 0 us
  Pallas kernels: 0 us -> 81.8 us
  blocking collectives: 43.6 us -> 0 us
  matrix products: 24.1 us -> 5.77 us
  between operations: 13.9 us -> 0.84 us
  other arithmetic: 20.2 us -> 12 us
  starting transfers between devices: 6.6 us -> 0 us
    reduce_scatter x3 -> x0, waiting for transfers between devices: 123 us -> none  [the longest x1 55.1 us: body(): lax.psum_scatter(jnp.dot(block_rows, joined, preferred_element_type=jnp.f...]
    all_gather x1 -> x0, waiting for transfers between devices: 116 us -> none  [body(): lax.all_gather(w_out, 'kv', axis=1, tiled=True)]
    pallas_call x0 -> x2, Pallas kernels: none -> 81.8 us  [the longest x1 42.9 us: tail(): pl.pallas_call(functools.partial(tail_kernel, kv, tp), out_shape=jax.Shap...]
    all_gather x2 -> x0, blocking collectives: 37.8 us -> none  [the longest x1 31.1 us: body(): lax.all_gather(mlp_input, 'kv', axis=0, tiled=True)]
    dot_general x4 -> x0, matrix products: 16.5 us -> none  [the longest x1 5.24 us: body(): jnp.dot(mixed, lax.all_gather(w_out, 'kv', axis=1, tiled=True), preferred...]
    psum x1 -> x0, waiting for transfers between devices: 14.4 us -> none  [body(): lax.psum(up_partial.astype(jnp.float32).astype(jnp.bfloat16), 'tp')]
    all_to_all x1 -> x0, starting transfers between devices: 6.22 us -> none  [body(): lax.all_to_all(normed, 'kv', split_axis=1, concat_axis=0, tiled=True)]
    psum x1 -> x0, blocking collectives: 5.76 us -> none  [body(): total_squares = lax.psum(jnp.sum(resid_float * resid_float, axis=-1), 'tp')]
  transfers between devices with their start and end apart: 6 -> 0, of which waited for: 5 -> 0; matrix products, arithmetic and copies ran while one was open for 15% -> 0% of each run, Pallas kernels for 0% -> 0%
where the time goes in v1:
time: 137 us; the launch traced here: 136 us
  Pallas kernels  81.8 us (60%)
  local copies, waits for them, and re-layouts  35.6 us (26%)
  other arithmetic  12 us (9%)
  matrix products  5.77 us (4%)
    pallas_call x1, Pallas kernels, tail(): pl.pallas_call(functools.partial(tail_kernel, kv, tp), out_shape=jax.Shap...  42.9 us
    pallas_call x1, Pallas kernels, project(): pl.pallas_call(functools.partial(project_kernel, kv, tp), out_shape=[jax....  38.9 us
    unnamed x33, local copies, waits for them, and re-layouts  33.5 us
    add x1, other arithmetic, body(): jnp.exp(log_decay)[..., None] * carried  9.66 us
    dot_general x1, matrix products, body(): jnp.einsum('bhk,bhkv->bhv', query_heads, new_state, precision=lax.Precisi...  5.77 us

profile of v1, /device:TPU:0, one launch (start us, length us, event | category | flops | bytes accessed | tf_op | source)
XLA Modules:
  0.0 136.0 jit_solution(4414763420414020578)
XLA Ops:
  0.6 0.7 reshape.49.g_ref
  1.4 1.2 copy-done.2
  2.6 1.2 copy-done.3
  3.8 1.0 copy-done.5
  4.8 1.0 copy-done.6
  5.9 1.0 copy-done.7
  6.9 0.8 copy-done.8
  7.7 38.9 %project.1 = (bf16[16,512]{1,0:T(8,128)(2,1)S(1)}, bf16[16,512]{1,0:T(8,128)(2,1)S(1)}, bf16[16,512]{1,0:T(8,128)(2,1)S(1)}, bf16[16,1024]{1,0:T(8,128)(2,1)S(1)}, bf16[16,1024]{1,0:T(8,128)(2,1)S(1)}) custom-call(bf16[16,1024]{1,0:T(8,128)(2,1)S(1)} %copy-done.8, bf16[1,4096]{1,0:T(2,128)(2,1)S(1)} %reshape.49.g_ref, bf16[512,512]{1,0:T(8,128)(2,1)S(1)} %copy-done.5, ...), custom_call_target="tpu_custom_call" | custom-call | tf_op jit(solution)/shard_map/project/pallas_call | solution.py:137
  46.6 0.7 fusion.10
  47.5 5.9 %copy.18 = f32[2,8,512,256]{3,2,1,0:T(8,128)S(1)} copy(f32[2,8,512,256]{3,1,2,0:T(8,128)} %bitcast.28) | data formatting | bytes 16777216
  53.3 0.0 copy-start.11
  53.4 5.8 %fusion = f32[16,4,1,256]{3,2,1,0:T(1,128)S(1)} fusion(f32[16,4,128,1]{2,3,1,0:T(1,128)S(1)} %bitcast.33, f32[16,4,128,256]{3,2,1,0:T(8,128)S(1)} %bitcast.26, f32[16,4,128]{2,1,0:T(4,128)S(1)} %exp.21, f32[16,4,256]{2,1,0:T(4,128)S(1)} %reshape.56, f32[16,4,128]{2,1,0:T(4,128)S(1)} %reshape.55), kind=kOutput, calls=%fused_computation.1 | convolution fusion | flops 31457280 | bytes 8617984 | tf_op jit(solution)/shard_map/bhk,bhkv->bhv/dot_general | solution.py:390
  59.1 0.1 fusion.5
  59.3 0.1 fusion.7
  59.5 2.2 %copy-done = bf16[1024,2048]{1,0:T(8,128)(2,1)S(1)} copy-done((bf16[1024,2048]{1,0:T(8,128)(2,1)S(1)}, bf16[1024,2048]{1,0:T(8,128)(2,1)}, u32[]{:S(2)}) %copy-start) | copy-done | bytes 4194328
  61.7 2.2 %copy-done.1 = bf16[2048,1024]{1,0:T(8,128)(2,1)S(1)} copy-done((bf16[2048,1024]{1,0:T(8,128)(2,1)S(1)}, bf16[2048,1024]{1,0:T(8,128)(2,1)}, u32[]{:S(2)}) %copy-start.1) | copy-done | bytes 4194328
  63.9 42.9 %tail.1 = bf16[16,1024]{1,0:T(8,128)(2,1)S(1)} custom-call(bf16[16,1024]{1,0:T(8,128)(2,1)S(1)} %bitcast.24, bf16[16,1024]{1,0:T(8,128)(2,1)S(1)} %copy-done.9, bf16[1,1024]{1,0:T(2,128)(2,1)S(1)} %reshape.54.g_ref, bf16[1024,512]{1,0:T(8,128)(2,1)S(1)} %copy-done.4, bf16[1024,2048]{1,0:T(8,128)(2,1)S(1)} %copy-done, bf16[2048,1024]{1,0:T(8,128)(2,1)S(1)} %copy-done.1), custom_call_target="tpu_custom_call" | custom-call | tf_op jit(solution)/shard_map/tail/pallas_call | solution.py:311
  106.7 1.4 %broadcast_multiply_fusion = f32[16,4,128,256]{3,2,1,0:T(8,128)S(1)} fusion(f32[16,4,256]{2,1,0:T(4,128)S(1)} %reshape.56, f32[16,4,128]{2,1,0:T(4,128)S(1)} %reshape.55), kind=kLoop, calls=%fused_computation.4 | loop fusion | flops 2097152 | bytes 8486912 | tf_op jit(solution)/shard_map/mul | solution.py:387
  108.2 8.3 %copy.21 = f32[2,8,512,256]{3,1,2,0:T(8,128)} copy(f32[2,8,512,256]{3,2,1,0:T(8,128)S(1)} %bitcast.25) | data formatting | bytes 16777216
  116.4 1.2 mul.78
  117.7 0.0 slice-start.1
  117.7 8.1 %copy.20 = f32[2,8,512,256]{3,1,2,0:T(8,128)} copy(f32[2,8,512,256]{3,2,1,0:T(8,128)S(1)} %bitcast.27) | data formatting | bytes 16777216
  125.7 9.7 %multiply_add_fusion = f32[16,131072]{1,0:T(8,128)} fusion(f32[16,131072]{1,0:T(8,128)} %bitcast.31, f32[16,131072]{1,0:T(8,128)} %bitcast.32, f32[16,131072]{1,0:T(8,128)S(1)} %bitcast.30), kind=kLoop, calls=%fused_computation | loop fusion | flops 4194304 | bytes 33554432 | tf_op jit(solution)/shard_map/add | solution.py:387
  135.4 0.6 copy.25
  (28 shorter events, 0.2 us)
Async XLA Ops:
  1.3 1.2 copy-start.2
  2.6 1.2 copy-start.3
  3.8 1.0 copy-start.5
  4.8 1.0 copy-start.6
  5.9 1.0 copy-start.7
  6.9 0.8 copy-start.8
  53.3 6.0 %copy-start.11 = (bf16[256]{0:T(256)(128)(2,1)S(1)}, bf16[256]{0:T(256)(128)(2,1)}, u32[]{:S(2)}) copy-start(bf16[256]{0:T(256)(128)(2,1)} %param.23) | copy-start | bytes 1540
  53.3 6.1 %copy-start.10 = (bf16[1024]{0:T(1024)(128)(2,1)S(1)}, bf16[1024]{0:T(1024)(128)(2,1)}, u32[]{:S(2)}) copy-start(bf16[1024]{0:T(1024)(128)(2,1)} %param.25) | copy-start | bytes 6148
  53.3 6.1 %copy-start.4 = (bf16[1024,512]{1,0:T(8,128)(2,1)S(1)}, bf16[1024,512]{1,0:T(8,128)(2,1)}, u32[]{:S(2)}) copy-start(bf16[1024,512]{1,0:T(8,128)(2,1)} %wo.1) | copy-start | bytes 3145732
  53.4 6.1 %copy-start.9 = (bf16[16,1024]{1,0:T(8,128)(2,1)S(1)}, bf16[16,1024]{1,0:T(8,128)(2,1)}, u32[]{:S(2)}) copy-start(bf16[16,1024]{1,0:T(8,128)(2,1)} %h_ref.3) | copy-start | bytes 98308
  59.5 2.2 %copy-start = (bf16[1024,2048]{1,0:T(8,128)(2,1)S(1)}, bf16[1024,2048]{1,0:T(8,128)(2,1)}, u32[]{:S(2)}) copy-start(bf16[1024,2048]{1,0:T(8,128)(2,1)} %wu.1) | copy-start | bytes 12582916
  61.7 2.2 %copy-start.1 = (bf16[2048,1024]{1,0:T(8,128)(2,1)S(1)}, bf16[2048,1024]{1,0:T(8,128)(2,1)}, u32[]{:S(2)}) copy-start(bf16[2048,1024]{1,0:T(8,128)(2,1)} %wd.1) | copy-start | bytes 12582916
  116.4 9.3 %slice-start = ((s8[8388608]{0:T(1024)(128)(4,1)}), s8[4194304]{0:T(1024)(128)(4,1)S(1)}, s32[]{:S(2)}) async-start(s8[8388608]{0:T(1024)(128)(4,1)} %bitcast.29), calls=%async_computation | async-start | bytes 8388608
  117.7 8.1 %slice-start.1 = ((s8[8388608]{0:T(1024)(128)(4,1)}), s8[4194304]{0:T(1024)(128)(4,1)S(1)}, s32[]{:S(2)}) async-start(s8[8388608]{0:T(1024)(128)(4,1)} %bitcast.29), calls=%async_computation.1 | async-start | bytes 8388608

commit v2 on v1

--- a/solution.py
+++ b/solution.py
@@ -33,18 +33,31 @@
     return jnp.dot(a, b, preferred_element_type=F32)
 
 
+def inner_size(kv):
+    size = 1
+    while (size * 2) ** 2 <= kv:
+        size = size * 2
+    return size
+
+
 def project_kernel(
     kv, tp, h_ref, g_ref, w0, w1, w2, w3, w4, o0, o1, o2, o3, o4,
     xbuf, v0, v1, v2, v3, v4, s0, s1, s2, s3, s4, r0, r1, r2, r3, r4,
-    ssq, wsem, xs_sem, xr_sem, ss_sem, sr_sem, ps_sem, pr_sem,
+    t0, t1, t2, t3, t4, u0, u1, u2, u3, u4,
+    ssq, wsem, xs_sem, xr_sem, ss_sem, sr_sem, ps_sem, pr_sem, qs_sem, qr_sem,
 ):
     i, j = lax.axis_index("kv"), lax.axis_index("tp")
+    ny = inner_size(kv)
+    nz = kv // ny
+    z, y = i // ny, lax.rem(i, ny)
     ratio = kv // tp
     rows = h_ref.shape[0]
     width = xbuf.shape[2]
     owner = i // ratio
     ws, vs, outs = (w0, w1, w2, w3, w4), (v0, v1, v2, v3, v4), (o0, o1, o2, o3, o4)
     sends, recvs = (s0, s1, s2, s3, s4), (r0, r1, r2, r3, r4)
+    sums, finals = (t0, t1, t2, t3, t4), (u0, u1, u2, u3, u4)
+    order = (3, 4, 1, 0, 2)
     loads = [pltpu.make_async_copy(w, v, wsem.at[n]) for n, (w, v) in enumerate(zip(ws, vs))]
 
     hidden_sends = []
@@ -61,8 +74,8 @@
             copy.start()
         else:
             pl.when(dst_i != i)(copy.start)
-    for load in loads:
-        load.start()
+    for n in order:
+        loads[n].start()
 
     hidden = h_ref[...].astype(F32)
     ssq[j] = jnp.broadcast_to(jnp.sum(hidden * hidden, axis=1, keepdims=True), (rows, 128))
@@ -88,20 +101,38 @@
     gain = g_ref[:, pl.ds(pl.multiple_of(i * width, 128), width)].astype(F32)
     x = (xbuf[...].reshape(kv * rows, width).astype(F32) * gain).astype(BF16)
     part_sends = []
-    for n in range(5):
+    for n in order:
         loads[n].wait()
         part = dot(x, vs[n][...]).astype(BF16)
-        sends[n][...] = part.reshape(sends[n].shape)
-        for s in range(1, kv):
-            k = lax.rem(i + s, kv)
+        for zz in range(nz):
+            for yy in range(ny):
+                low = (zz * ny + yy) * rows
+                sends[n][yy, zz] = part[low : low + rows]
+        for s in range(1, ny):
+            yy = lax.rem(y + s, ny)
             copy = remote(
-                sends[n].at[k], recvs[n].at[i], ps_sem.at[n, s], pr_sem.at[n, i], k, j
+                sends[n].at[yy], recvs[n].at[y], ps_sem.at[n, s], pr_sem.at[n, y], z * ny + yy, j
             )
             copy.start()
             part_sends.append(copy)
-        if n == 0:
-            for copy in square_sends:
-                copy.start()
+    for copy in square_sends:
+        copy.start()
+    for n in order:
+        acc = sends[n][y].astype(F32)
+        for s in range(1, ny):
+            yy = lax.rem(y + s, ny)
+            remote(
+                recvs[n].at[yy], recvs[n].at[yy], ps_sem.at[n, 0], pr_sem.at[n, yy], z * ny + yy, j
+            ).wait_recv()
+            acc = acc + recvs[n][yy].astype(F32)
+        sums[n][...] = acc.astype(BF16)
+        for s in range(1, nz):
+            zz = lax.rem(z + s, nz)
+            copy = remote(
+                sums[n].at[zz], finals[n].at[z], qs_sem.at[n, s], qr_sem.at[n, z], zz * ny + y, j
+            )
+            copy.start()
+            part_sends.append(copy)
     for s in range(1, tp):
         k = lax.rem(j + s, tp)
         remote(ssq.at[k], ssq.at[k], ss_sem.at[0], sr_sem.at[k], i, k).wait_recv()
@@ -109,14 +140,14 @@
     for s in range(1, tp):
         total = total + ssq[s]
     scale = lax.rsqrt(total[:, :1] / (kv * width) + epsilon)
-    for n in range(5):
-        acc = sends[n][i].astype(F32)
-        for s in range(1, kv):
-            k = lax.rem(i + s, kv)
+    for n in order:
+        acc = sums[n][z].astype(F32)
+        for s in range(1, nz):
+            zz = lax.rem(z + s, nz)
             remote(
-                recvs[n].at[k], recvs[n].at[k], ps_sem.at[n, 0], pr_sem.at[n, k], k, j
+                finals[n].at[zz], finals[n].at[zz], qs_sem.at[n, 0], qr_sem.at[n, zz], zz * ny + y, j
             ).wait_recv()
-            acc = acc + recvs[n][k].astype(F32)
+            acc = acc + finals[n][zz].astype(F32)
         outs[n][...] = (acc * scale).astype(BF16)
     for a, s, dst_i, copy in hidden_sends:
         if s:
@@ -130,9 +161,12 @@
 def project(kv, tp, hidden_rows, norm_gain, weights):
     rows = hidden_rows.shape[0]
     width = weights[0].shape[0]
+    ny = inner_size(kv)
+    nz = kv // ny
     vmem = pl.BlockSpec(memory_space=pltpu.VMEM)
     anywhere = pl.BlockSpec(memory_space=pl.ANY)
-    slots = [pltpu.VMEM((kv, rows, w.shape[1]), BF16) for w in weights]
+    slots = [pltpu.VMEM((ny, nz, rows, w.shape[1]), BF16) for w in weights]
+    lines = [pltpu.VMEM((nz, rows, w.shape[1]), BF16) for w in weights]
     dma = pltpu.SemaphoreType.DMA
     return pl.pallas_call(
         functools.partial(project_kernel, kv, tp),
@@ -143,6 +177,8 @@
         + [pltpu.VMEM(w.shape, BF16) for w in weights]
         + slots
         + slots
+        + lines
+        + lines
         + [
             pltpu.VMEM((tp, rows, 128), F32),
             dma((5,)),
@@ -150,14 +186,86 @@
             dma((kv,)),
             dma((tp,)),
             dma((tp,)),
-            dma((5, kv)),
-            dma((5, kv)),
+            dma((5, ny)),
+            dma((5, ny)),
+            dma((5, nz)),
+            dma((5, nz)),
         ],
         compiler_params=pltpu.CompilerParams(
-            has_side_effects=True, vmem_limit_bytes=32 * 1024 * 1024
+            has_side_effects=True, vmem_limit_bytes=62 * 1024 * 1024
         ),
         name="project",
     )(hidden_rows, norm_gain.reshape(1, -1), *weights)
+
+
+PARTS = 2
+CHUNKS = 2
+
+
+def state_kernel(
+    q_ref, k_ref, d_ref, v_ref, g_ref, bias_ref, gain_ref, old_ref, new_ref, mixed_ref,
+    query, key, decay, total,
+):
+    part = pl.program_id(1)
+    channels = DK // PARTS
+
+    @pl.when(part == 0)
+    def _():
+        pre = d_ref[...].astype(F32) + bias_ref[...]
+        log_decay = jnp.minimum(pre, 0.0) - jnp.log1p(jnp.exp(-jnp.abs(pre)))
+        decay[...] = jnp.exp(log_decay / decay_normalizer)
+        query[...] = q_ref[...].astype(F32) * DK ** (-0.5)
+        key[...] = k_ref[...].astype(F32)
+        total[...] = jnp.zeros_like(total)
+
+    value = v_ref[...].astype(F32)
+    acc = total[...]
+    q, k, d = query[...], key[...], decay[...]
+    for c in range(channels):
+        at = slice(c * DV, (c + 1) * DV)
+        new = d[:, c : c + 1] * old_ref[:, at] + k[:, c : c + 1] * value
+        new_ref[:, at] = new
+        acc = acc + q[:, c : c + 1] * new
+    total[...] = acc
+    query[...] = pltpu.roll(q, DK - channels, 1)
+    key[...] = pltpu.roll(k, DK - channels, 1)
+    decay[...] = pltpu.roll(d, DK - channels, 1)
+
+    @pl.when(part == PARTS - 1)
+    def _():
+        gate = g_ref[...].astype(F32)
+        mixed = acc * lax.rsqrt(jnp.mean(acc * acc, axis=1, keepdims=True) + epsilon)
+        mixed_ref[...] = (mixed * gain_ref[...].astype(F32) * jax.nn.silu(gate)).astype(BF16)
+
+
+def state(queries, keys_new, decay_pre, values, out_gate, decay_bias, head_gain, carried):
+    rows, total = carried.shape
+    heads = total // (DK * DV)
+    narrow = pl.BlockSpec((rows, DK), lambda h, p: (0, h))
+    wide = pl.BlockSpec((rows, DV), lambda h, p: (0, h))
+    block = pl.BlockSpec((rows, DK * DV // PARTS), lambda h, p: (0, h * PARTS + p))
+    return pl.pallas_call(
+        state_kernel,
+        grid=(heads, PARTS),
+        out_shape=[
+            jax.ShapeDtypeStruct(carried.shape, F32),
+            jax.ShapeDtypeStruct((rows, heads * DV), BF16),
+        ],
+        in_specs=[narrow] * 3
+        + [wide] * 2
+        + [
+            pl.BlockSpec((1, DK), lambda h, p: (0, h)),
+            pl.BlockSpec((1, DV), lambda h, p: (0, 0)),
+            block,
+        ],
+        out_specs=[block, wide],
+        scratch_shapes=[pltpu.VMEM((rows, DK), F32)] * 3 + [pltpu.VMEM((rows, DV), F32)],
+        compiler_params=pltpu.CompilerParams(vmem_limit_bytes=62 * 1024 * 1024),
+        name="state",
+    )(
+        queries, keys_new, decay_pre, values, out_gate,
+        decay_bias.reshape(1, -1), head_gain.reshape(1, -1), carried,
+    )
 
 
 def tail_kernel(
@@ -245,37 +353,57 @@
     x = (rall[...].reshape(kv * rows, columns).astype(F32) * g_ref[...].astype(F32)).astype(BF16)
 
     half = vu.shape[1] // 2
+    piece = half // CHUNKS
     core, across = lax.rem(j, 2), j // 2
     other = 1 - core
     partner = across * 2 + other
-    usend[...] = dot(x, vu[:, pl.ds(pl.multiple_of(other * half, 128), half)]).astype(BF16)
-    give = remote(usend, urecv, us_sem, ur_sem, i, partner)
-    give.start()
-    mine = dot(x, vu[:, pl.ds(pl.multiple_of(core * half, 128), half)])
-    give.wait_recv()
-    mine = (mine + urecv[...].astype(F32)).astype(BF16)
-    xsend[...] = mine
-    for s in range(1, tp // 2):
-        to = lax.rem(across + s, tp // 2)
+
+    def columns_of(h, c):
+        return pl.ds(pl.multiple_of(h * half + c * piece, 128), piece)
+
+    for c in range(CHUNKS):
+        usend[c] = dot(x, vu[:, columns_of(other, c)]).astype(BF16)
+        copy = remote(usend.at[c], urecv.at[c], us_sem.at[c], ur_sem.at[c], i, partner)
+        copy.start()
+        sent.append(copy)
+    for c in range(CHUNKS):
+        mine = dot(x, vu[:, columns_of(core, c)])
+        remote(urecv.at[c], urecv.at[c], us_sem.at[c], ur_sem.at[c], i, partner).wait_recv()
+        xsend[c] = (mine + urecv[c].astype(F32)).astype(BF16)
+        for s in range(1, tp // 2):
+            to = lax.rem(across + s, tp // 2)
+            copy = remote(
+                xsend.at[c],
+                xrecv.at[across, c],
+                xs_sem.at[s, c],
+                xr_sem.at[across, c],
+                i,
+                to * 2 + core,
+            )
+            copy.start()
+            sent.append(copy)
+    loads[2].wait()
+    down = None
+    for c in range(CHUNKS):
+        total = xsend[c].astype(F32)
+        for s in range(1, tp // 2):
+            at = lax.rem(across + s, tp // 2)
+            slot_ref = xrecv.at[at, c]
+            remote(
+                slot_ref, slot_ref, xs_sem.at[0, c], xr_sem.at[at, c], i, at * 2 + core
+            ).wait_recv()
+            total = total + xrecv[at, c].astype(F32)
+        act[core, c] = jnp.square(jnp.maximum(total, 0.0)).astype(BF16)
         copy = remote(
-            xsend, xrecv.at[across], xs_sem.at[s], xr_sem.at[across], i, to * 2 + core
+            act.at[core, c], act.at[core, c], as_sem.at[c], ar_sem.at[core, c], i, partner
         )
         copy.start()
         sent.append(copy)
-    loads[2].wait()
-    total = xsend[...].astype(F32)
-    for s in range(1, tp // 2):
-        at = lax.rem(across + s, tp // 2)
-        remote(
-            xrecv.at[at], xrecv.at[at], xs_sem.at[0], xr_sem.at[at], i, at * 2 + core
-        ).wait_recv()
-        total = total + xrecv[at].astype(F32)
-    act[core] = jnp.square(jnp.maximum(total, 0.0)).astype(BF16)
-    share = remote(act.at[core], act.at[core], as_sem, ar_sem.at[core], i, partner)
-    share.start()
-    down = dot(act[core], vd[pl.ds(pl.multiple_of(core * half, 128), half), :])
-    remote(act.at[other], act.at[other], as_sem, ar_sem.at[other], i, partner).wait_recv()
-    down = down + dot(act[other], vd[pl.ds(pl.multiple_of(other * half, 128), half), :])
+        term = dot(act[core, c], vd[columns_of(core, c), :])
+        down = term if down is None else down + term
+        arrive = act.at[other, c]
+        remote(arrive, arrive, as_sem.at[c], ar_sem.at[other, c], i, partner).wait_recv()
+        down = down + dot(act[other, c], vd[columns_of(other, c), :])
     dsend[...] = down.astype(BF16).reshape(dsend.shape)
     everyone(lambda k: dsend.at[k], drecv, ds_sem, dr_sem)
 
@@ -292,8 +420,6 @@
         acc = acc + drecv[k].astype(F32)
     acc = (acc * (scale * scale)).astype(BF16)
     out_ref[...] = (resid[...].astype(F32) + acc.astype(F32)).astype(BF16)
-    give.wait_send()
-    share.wait_send()
     pl.when(owner != j)(own_send.wait_send)
     for copy in sent:
         copy.wait_send()
@@ -323,11 +449,11 @@
             pltpu.VMEM((rows, columns), BF16),
             pltpu.VMEM((kv, rows, columns), BF16),
             pltpu.VMEM((tp, rows, 128), F32),
-            pltpu.VMEM((everything, half), BF16),
-            pltpu.VMEM((everything, half), BF16),
-            pltpu.VMEM((everything, half), BF16),
-            pltpu.VMEM((tp // 2, everything, half), BF16),
-            pltpu.VMEM((2, everything, half), BF16),
+            pltpu.VMEM((CHUNKS, everything, half // CHUNKS), BF16),
+            pltpu.VMEM((CHUNKS, everything, half // CHUNKS), BF16),
+            pltpu.VMEM((CHUNKS, everything, half // CHUNKS), BF16),
+            pltpu.VMEM((tp // 2, CHUNKS, everything, half // CHUNKS), BF16),
+            pltpu.VMEM((2, CHUNKS, everything, half // CHUNKS), BF16),
             pltpu.VMEM((kv, rows, columns), BF16),
             pltpu.VMEM((kv, rows, columns), BF16),
             dma((3,)),
@@ -339,17 +465,17 @@
             dma((kv,)),
             dma((tp,)),
             dma((tp,)),
-            dma(()),
-            dma(()),
-            dma((tp // 2,)),
-            dma((tp // 2,)),
-            dma(()),
-            dma((2,)),
+            dma((CHUNKS,)),
+            dma((CHUNKS,)),
+            dma((tp // 2, CHUNKS)),
+            dma((tp // 2, CHUNKS)),
+            dma((CHUNKS,)),
+            dma((2, CHUNKS)),
             dma((kv,)),
             dma((kv,)),
         ],
         compiler_params=pltpu.CompilerParams(
-            has_side_effects=True, vmem_limit_bytes=32 * 1024 * 1024
+            has_side_effects=True, vmem_limit_bytes=62 * 1024 * 1024
         ),
         name="tail",
     )(mixed, hidden_rows, mlp_gain.reshape(1, -1), w_out, w_up, w_down)
@@ -373,27 +499,14 @@
     w_up,
     w_down,
 ):
-    seq_rows = hidden_rows.shape[0]
-    heads_here = decay_bias.shape[0] // DK
     queries, keys_new, decay_pre, values, out_gate = project(
         kv, tp, hidden_rows, norm_gain, (w_query, w_key, w_decay, w_value, w_gate)
     )
-    log_decay = jax.nn.log_sigmoid(decay_pre.astype(F32) + decay_bias) / decay_normalizer
-    log_decay = log_decay.reshape(seq_rows, heads_here, DK)
-    carried = carried_state.reshape(seq_rows, heads_here, DK, DV)
-    key_heads = keys_new.astype(F32).reshape(seq_rows, heads_here, DK)
-    value_heads = values.astype(F32).reshape(seq_rows, heads_here, DV)
-    new_state = (
-        jnp.exp(log_decay)[..., None] * carried + key_heads[..., None] * value_heads[..., None, :]
+    new_state, mixed = state(
+        queries, keys_new, decay_pre, values, out_gate, decay_bias, head_gain, carried_state
     )
-    query_heads = queries.astype(F32).reshape(seq_rows, heads_here, DK) * DK ** (-0.5)
-    head_out = jnp.einsum("bhk,bhkv->bhv", query_heads, new_state, precision=lax.Precision.HIGHEST)
-    gate_heads = out_gate.astype(F32).reshape(seq_rows, heads_here, DV)
-    mixed = head_out * lax.rsqrt(jnp.mean(head_out * head_out, axis=-1, keepdims=True) + epsilon)
-    mixed = (mixed * head_gain.astype(F32) * jax.nn.silu(gate_heads)).astype(BF16)
-    mixed = mixed.reshape(seq_rows, heads_here * DV)
     updated_rows = tail(kv, tp, mixed, hidden_rows, mlp_gain, w_out, w_up, w_down)
-    return (updated_rows, new_state.reshape(seq_rows, heads_here * DK * DV))
+    return (updated_rows, new_state)
 
 
 def solution(mesh):

time: 137 us -> 95.1 us (0.69)
  local copies, waits for them, and re-layouts: 35.6 us -> 4.51 us
  other arithmetic: 12 us -> 0 us
  Pallas kernels: 81.8 us -> 89.3 us
  matrix products: 5.77 us -> 0 us
    unnamed x33 -> x3, local copies, waits for them, and re-layouts: 33.5 us -> 1.38 us
    pallas_call x0 -> x1, Pallas kernels: none -> 10.7 us  [state(): pl.pallas_call(state_kernel, grid=(heads, PARTS), out_shape=[jax.ShapeDty...]
    add x1 -> x0, other arithmetic: 9.66 us -> none  [body(): jnp.exp(log_decay)[..., None] * carried]
    dot_general x1 -> x0, matrix products: 5.77 us -> none  [body(): jnp.einsum('bhk,bhkv->bhv', query_heads, new_state, precision=lax.Precisi...]
    pallas_call x1, Pallas kernels: 38.9 us -> 35.8 us  [project(): pl.pallas_call(functools.partial(project_kernel, kv, tp), out_shape=[jax....]
    mul x1 -> x0, other arithmetic: 1.44 us -> none  [body(): key_heads[..., None] * value_heads[..., None, :]]
where the time goes in v2:
time: 95.1 us; the launch traced here: 94.5 us
  Pallas kernels  89.3 us (94%)
  local copies, waits for them, and re-layouts  4.51 us (5%)
    pallas_call x1, Pallas kernels, tail(): pl.pallas_call(functools.partial(tail_kernel, kv, tp), out_shape=jax.Shap...  42.8 us
    pallas_call x1, Pallas kernels, project(): pl.pallas_call(functools.partial(project_kernel, kv, tp), out_shape=[jax....  35.8 us
    pallas_call x1, Pallas kernels, state(): pl.pallas_call(state_kernel, grid=(heads, PARTS), out_shape=[jax.ShapeDty...  10.7 us

profile of v2, /device:TPU:0, one launch (start us, length us, event | category | flops | bytes accessed | tf_op | source)
XLA Modules:
  0.0 94.5 jit_solution(11930301155106928264)
XLA Ops:
  0.6 0.0 copy-start
  0.6 1.3 %reshape.16.g_ref = bf16[1,4096]{1,0:T(2,128)(2,1)} reshape(bf16[4096]{0:T(1024)(128)(2,1)} %param.16) | data formatting | bytes 16384 | tf_op jit(solution)/shard_map/reshape | solution.py:198
  2.0 35.8 %project.1 = (bf16[16,512]{1,0:T(8,128)(2,1)}, bf16[16,512]{1,0:T(8,128)(2,1)}, bf16[16,512]{1,0:T(8,128)(2,1)}, bf16[16,1024]{1,0:T(8,128)(2,1)}, bf16[16,1024]{1,0:T(8,128)(2,1)}) custom-call(bf16[16,1024]{1,0:T(8,128)(2,1)} %h_ref.3, bf16[1,4096]{1,0:T(2,128)(2,1)} %reshape.16.g_ref, bf16[512,512]{1,0:T(8,128)(2,1)} %w0.1, bf16[512,512]{1,0:T(8,128)(2,1)} %w1.1, ...), custom_call_target="tpu_custom_call" | custom-call | tf_op jit(solution)/shard_map/project/pallas_call | solution.py:171
  37.8 1.2 %reshape.18.gain_ref = bf16[1,256]{1,0:T(2,128)(2,1)} reshape(bf16[256]{0:T(256)(128)(2,1)} %param.23) | data formatting | bytes 1024 | tf_op jit(solution)/shard_map/reshape | solution.py:267
  39.0 10.7 %state.1 = (f32[16,131072]{1,0:T(8,128)}, bf16[16,1024]{1,0:T(8,128)(2,1)}) custom-call(bf16[16,512]{1,0:T(8,128)(2,1)} %get-tuple-element.9.q_ref, bf16[16,512]{1,0:T(8,128)(2,1)} %get-tuple-element.10.k_ref, bf16[16,512]{1,0:T(8,128)(2,1)} %get-tuple-element.11.d_ref, bf16[16,1024]{1,0:T(8,128)(2,1)} %get-tuple-element.12.v_ref, ...), custom_call_target="tpu_custom_call" | custom-call | tf_op jit(solution)/shard_map/state/pallas_call | solution.py:247
  49.7 0.0 copy-done
  49.7 0.6 reshape.19.g_ref
  50.3 42.8 %tail.1 = bf16[16,1024]{1,0:T(8,128)(2,1)} custom-call(bf16[16,1024]{1,0:T(8,128)(2,1)} %get-tuple-element.14.mixed_ref, bf16[16,1024]{1,0:T(8,128)(2,1)} %h_ref.3, bf16[1,1024]{1,0:T(2,128)(2,1)} %reshape.19.g_ref, bf16[1024,512]{1,0:T(8,128)(2,1)} %wo.1, bf16[1024,2048]{1,0:T(8,128)(2,1)} %wu.1, bf16[2048,1024]{1,0:T(8,128)(2,1)} %wd.1), custom_call_target="tpu_custom_call" | custom-call | tf_op jit(solution)/shard_map/tail/pallas_call | solution.py:437
  93.1 1.4 %copy.17 = bf16[16,1024]{1,0:T(8,128)(2,1)} copy(bf16[16,1024]{1,0:T(8,128)(2,1)} %tail.1) | data formatting | bytes 65536
Async XLA Ops:
  0.6 49.1 %copy-start = (bf16[1024]{0:T(1024)(128)(2,1)S(1)}, bf16[1024]{0:T(1024)(128)(2,1)}, u32[]{:S(2)}) copy-start(bf16[1024]{0:T(1024)(128)(2,1)} %param.25) | copy-start | bytes 6148

commit v3 on v2

--- a/solution.py
+++ b/solution.py
@@ -199,7 +199,7 @@
 
 
 PARTS = 2
-CHUNKS = 2
+CHUNKS = 4
 
 
 def state_kernel(
@@ -353,7 +353,8 @@
     x = (rall[...].reshape(kv * rows, columns).astype(F32) * g_ref[...].astype(F32)).astype(BF16)
 
     half = vu.shape[1] // 2
-    piece = half // CHUNKS
+    chunks = usend.shape[0]
+    piece = half // chunks
     core, across = lax.rem(j, 2), j // 2
     other = 1 - core
     partner = across * 2 + other
@@ -361,12 +362,16 @@
     def columns_of(h, c):
         return pl.ds(pl.multiple_of(h * half + c * piece, 128), piece)
 
-    for c in range(CHUNKS):
+    def give(c):
         usend[c] = dot(x, vu[:, columns_of(other, c)]).astype(BF16)
         copy = remote(usend.at[c], urecv.at[c], us_sem.at[c], ur_sem.at[c], i, partner)
         copy.start()
         sent.append(copy)
-    for c in range(CHUNKS):
+
+    give(0)
+    for c in range(chunks):
+        if c + 1 < chunks:
+            give(c + 1)
         mine = dot(x, vu[:, columns_of(core, c)])
         remote(urecv.at[c], urecv.at[c], us_sem.at[c], ur_sem.at[c], i, partner).wait_recv()
         xsend[c] = (mine + urecv[c].astype(F32)).astype(BF16)
@@ -384,7 +389,7 @@
             sent.append(copy)
     loads[2].wait()
     down = None
-    for c in range(CHUNKS):
+    for c in range(chunks):
         total = xsend[c].astype(F32)
         for s in range(1, tp // 2):
             at = lax.rem(across + s, tp // 2)
@@ -431,6 +436,7 @@
     ratio = kv // tp
     half = w_up.shape[1] // 2
     everything = kv * rows
+    chunks = max(1, min(CHUNKS, half // 128))
     vmem = pl.BlockSpec(memory_space=pltpu.VMEM)
     anywhere = pl.BlockSpec(memory_space=pl.ANY)
     dma = pltpu.SemaphoreType.DMA
@@ -449,11 +455,11 @@
             pltpu.VMEM((rows, columns), BF16),
             pltpu.VMEM((kv, rows, columns), BF16),
             pltpu.VMEM((tp, rows, 128), F32),
-            pltpu.VMEM((CHUNKS, everything, half // CHUNKS), BF16),
-            pltpu.VMEM((CHUNKS, everything, half // CHUNKS), BF16),
-            pltpu.VMEM((CHUNKS, everything, half // CHUNKS), BF16),
-            pltpu.VMEM((tp // 2, CHUNKS, everything, half // CHUNKS), BF16),
-            pltpu.VMEM((2, CHUNKS, everything, half // CHUNKS), BF16),
+            pltpu.VMEM((chunks, everything, half // chunks), BF16),
+            pltpu.VMEM((chunks, everything, half // chunks), BF16),
+            pltpu.VMEM((chunks, everything, half // chunks), BF16),
+            pltpu.VMEM((tp // 2, chunks, everything, half // chunks), BF16),
+            pltpu.VMEM((2, chunks, everything, half // chunks), BF16),
             pltpu.VMEM((kv, rows, columns), BF16),
             pltpu.VMEM((kv, rows, columns), BF16),
             dma((3,)),
@@ -465,12 +471,12 @@
             dma((kv,)),
             dma((tp,)),
             dma((tp,)),
-            dma((CHUNKS,)),
-            dma((CHUNKS,)),
-            dma((tp // 2, CHUNKS)),
-            dma((tp // 2, CHUNKS)),
-            dma((CHUNKS,)),
-            dma((2, CHUNKS)),
+            dma((chunks,)),
+            dma((chunks,)),
+            dma((tp // 2, chunks)),
+            dma((tp // 2, chunks)),
+            dma((chunks,)),
+            dma((2, chunks)),
             dma((kv,)),
             dma((kv,)),
         ],

time: 95.1 us -> 95.1 us (level)
  no operation moved by 1% of the time
where the time goes in v3:
time: 95.1 us; the launch traced here: 94.5 us
  Pallas kernels  89.3 us (94%)
  local copies, waits for them, and re-layouts  4.51 us (5%)
    pallas_call x1, Pallas kernels, tail(): pl.pallas_call(functools.partial(tail_kernel, kv, tp), out_shape=jax.Shap...  42.8 us
    pallas_call x1, Pallas kernels, project(): pl.pallas_call(functools.partial(project_kernel, kv, tp), out_shape=[jax....  35.8 us
    pallas_call x1, Pallas kernels, state(): pl.pallas_call(state_kernel, grid=(heads, PARTS), out_shape=[jax.ShapeDty...  10.7 us

profile of v3, /device:TPU:0, one launch (start us, length us, event | category | flops | bytes accessed | tf_op | source)
XLA Modules:
  0.0 94.5 jit_solution(11847631513680989599)
XLA Ops:
  0.6 0.0 copy-start
  0.6 1.3 %reshape.16.g_ref = bf16[1,4096]{1,0:T(2,128)(2,1)} reshape(bf16[4096]{0:T(1024)(128)(2,1)} %param.16) | data formatting | bytes 16384 | tf_op jit(solution)/shard_map/reshape | solution.py:198
  2.0 35.8 %project.1 = (bf16[16,512]{1,0:T(8,128)(2,1)}, bf16[16,512]{1,0:T(8,128)(2,1)}, bf16[16,512]{1,0:T(8,128)(2,1)}, bf16[16,1024]{1,0:T(8,128)(2,1)}, bf16[16,1024]{1,0:T(8,128)(2,1)}) custom-call(bf16[16,1024]{1,0:T(8,128)(2,1)} %h_ref.3, bf16[1,4096]{1,0:T(2,128)(2,1)} %reshape.16.g_ref, bf16[512,512]{1,0:T(8,128)(2,1)} %w0.1, bf16[512,512]{1,0:T(8,128)(2,1)} %w1.1, ...), custom_call_target="tpu_custom_call" | custom-call | tf_op jit(solution)/shard_map/project/pallas_call | solution.py:171
  37.8 1.2 %reshape.18.gain_ref = bf16[1,256]{1,0:T(2,128)(2,1)} reshape(bf16[256]{0:T(256)(128)(2,1)} %param.23) | data formatting | bytes 1024 | tf_op jit(solution)/shard_map/reshape | solution.py:267
  39.0 10.7 %state.1 = (f32[16,131072]{1,0:T(8,128)}, bf16[16,1024]{1,0:T(8,128)(2,1)}) custom-call(bf16[16,512]{1,0:T(8,128)(2,1)} %get-tuple-element.9.q_ref, bf16[16,512]{1,0:T(8,128)(2,1)} %get-tuple-element.10.k_ref, bf16[16,512]{1,0:T(8,128)(2,1)} %get-tuple-element.11.d_ref, bf16[16,1024]{1,0:T(8,128)(2,1)} %get-tuple-element.12.v_ref, ...), custom_call_target="tpu_custom_call" | custom-call | tf_op jit(solution)/shard_map/state/pallas_call | solution.py:247
  49.7 0.0 copy-done
  49.7 0.6 reshape.19.g_ref
  50.3 42.8 %tail.1 = bf16[16,1024]{1,0:T(8,128)(2,1)} custom-call(bf16[16,1024]{1,0:T(8,128)(2,1)} %get-tuple-element.14.mixed_ref, bf16[16,1024]{1,0:T(8,128)(2,1)} %h_ref.3, bf16[1,1024]{1,0:T(2,128)(2,1)} %reshape.19.g_ref, bf16[1024,512]{1,0:T(8,128)(2,1)} %wo.1, bf16[1024,2048]{1,0:T(8,128)(2,1)} %wu.1, bf16[2048,1024]{1,0:T(8,128)(2,1)} %wd.1), custom_call_target="tpu_custom_call" | custom-call | tf_op jit(solution)/shard_map/tail/pallas_call | solution.py:443
  93.1 1.4 %copy.17 = bf16[16,1024]{1,0:T(8,128)(2,1)} copy(bf16[16,1024]{1,0:T(8,128)(2,1)} %tail.1) | data formatting | bytes 65536
Async XLA Ops:
  0.6 49.1 %copy-start = (bf16[1024]{0:T(1024)(128)(2,1)S(1)}, bf16[1024]{0:T(1024)(128)(2,1)}, u32[]{:S(2)}) copy-start(bf16[1024]{0:T(1024)(128)(2,1)} %param.25) | copy-start | bytes 6148
